TPU v7x, 32 devices: a whole 2x2x4 slice. The times are simulated.
32 devices in a mesh: dp: 4 (over y, x), kv: 4 (over z), tp: 2 (over core).
Axes of the slice: x: 2, y: 2, z: 4, core: 2. Of those that a mesh axis runs over, the one named last changes fastest.
Arguments:
- tokens: bfloat16 [32, 4096], P('dp', ('kv', 'tp')), may hold values from -6 to 6
- w_query: bfloat16 [4096, 2, 1024], P(None, 'tp', 'kv'), may hold values from -0.09375 to 0.09375
- w_forget: bfloat16 [4096, 2, 1024], P(None, 'tp', 'kv'), may hold values from -0.09375 to 0.09375
- w_input: bfloat16 [4096, 2, 1024], P(None, 'tp', 'kv'), may hold values from -0.09375 to 0.09375
- w_output_gate: bfloat16 [4096, 2, 1024], P(None, 'tp', 'kv'), may hold values from -0.09375 to 0.09375
- gate_floor: float32 [2048], P('tp'), may hold values from 0 to 0.9
- head_gain: float32 [128], replicated, may hold values from 0.1 to 1.9
- w_out: bfloat16 [2048, 4096], P(None, ('kv', 'tp')), may hold values from -0.125 to 0.125
- mix_gain: float32 [4096], replicated, may hold values from 0.1 to 1.9
- ffn_gain: float32 [4096], replicated, may hold values from 0.1 to 1.9
- w_up: bfloat16 [4096, 16384], P(None, ('kv', 'tp')), may hold values from -0.09375 to 0.09375
- w_down: bfloat16 [16384, 4096], P(('kv', 'tp')), may hold values from -0.0625 to 0.0625
- state: float32 [32, 16, 128, 128], P(('dp', 'kv'), 'tp'), may hold values from -6 to 6
Outputs:
- mixed: bfloat16 [32, 4096], P('dp', ('kv', 'tp'))
- new_state: float32 [32, 16, 128, 128], P(('dp', 'kv'), 'tp')
All inputs are finite; a program needn't handle non-finite values.
Results may differ from a plain program's by a relative error of at most 0.014.
Values may be sent and summed in bfloat16 or wider, within the bound.
A program may use at most 128 MiB of HBM per device.

v0:
```python
import jax
import jax.numpy as jnp
from jax import lax
from jax.sharding import PartitionSpec as P

EPSILON = 1e-06


def rms_scale(values, gain):
    return values * lax.rsqrt(jnp.mean(values * values, axis=-1, keepdims=True) + EPSILON) * gain


def per_device(
    tokens,
    w_query,
    w_forget,
    w_input,
    w_output_gate,
    gate_floor,
    head_gain,
    w_out,
    mix_gain,
    ffn_gain,
    w_up,
    w_down,
    state,
):
    group_kv = lax.axis_size("kv")
    group_tp = lax.axis_size("tp")
    tokens_f = tokens.astype(jnp.float32)
    full_rows = lax.all_gather(tokens, ("kv", "tp"), axis=1, tiled=True)
    normed = rms_scale(full_rows.astype(jnp.float32), mix_gain).astype(jnp.bfloat16)

    def project(weight):
        return jnp.dot(normed, weight[:, 0, :], preferred_element_type=jnp.float32).astype(
            jnp.bfloat16
        )

    query_raw, forget_raw, input_raw, gate_raw = (
        lax.all_to_all(project(w_query), "kv", split_axis=0, concat_axis=1, tiled=True),
        lax.all_to_all(project(w_forget), "kv", split_axis=0, concat_axis=1, tiled=True),
        lax.all_to_all(project(w_input), "kv", split_axis=0, concat_axis=1, tiled=True),
        lax.all_to_all(project(w_output_gate), "kv", split_axis=0, concat_axis=1, tiled=True),
    )
    seq_local = state.shape[0]
    heads_local = state.shape[1]
    head_size = state.shape[2]
    query_vec = query_raw.astype(jnp.float32).reshape(
        seq_local, heads_local, head_size
    ) * head_size ** (-0.5)
    floor_heads = gate_floor.reshape(heads_local, head_size)
    forget_gate = floor_heads + (1.0 - floor_heads) * jax.nn.sigmoid(
        forget_raw.astype(jnp.float32).reshape(seq_local, heads_local, head_size)
    )
    input_vec = input_raw.astype(jnp.float32).reshape(seq_local, heads_local, head_size)
    gate_vec = gate_raw.astype(jnp.float32).reshape(seq_local, heads_local, head_size)
    new_state = (
        forget_gate[..., None] * state + (1.0 - forget_gate)[..., None] * input_vec[:, :, None, :]
    )
    head_out = jnp.einsum("bhk,bhkv->bhv", query_vec, new_state, precision=lax.Precision.HIGHEST)
    branch = rms_scale(head_out, head_gain) * jax.nn.silu(gate_vec)
    branch = branch.reshape(seq_local, 1, heads_local * head_size).astype(jnp.bfloat16)
    gathered = lax.all_gather(branch, ("kv", "tp"), axis=1, tiled=True)
    gathered = gathered.reshape(seq_local, group_kv, group_tp, heads_local * head_size)
    gathered = jnp.transpose(gathered, (1, 0, 2, 3)).reshape(
        group_kv * seq_local, group_tp * heads_local * head_size
    )
    projected = jnp.dot(gathered, w_out, preferred_element_type=jnp.float32)
    residual_one = (tokens_f + projected).astype(jnp.bfloat16)
    whole_rows = lax.all_gather(residual_one, ("kv", "tp"), axis=1, tiled=True)
    ffn_in = rms_scale(whole_rows.astype(jnp.float32), ffn_gain).astype(jnp.bfloat16)
    upward = jnp.dot(ffn_in, w_up, preferred_element_type=jnp.float32)
    hidden = jnp.square(jax.nn.relu(upward)).astype(jnp.bfloat16)
    partial_terms = jnp.dot(hidden, w_down, preferred_element_type=jnp.float32)
    summed = lax.psum_scatter(partial_terms, ("kv", "tp"), scatter_dimension=1, tiled=True)
    results = (residual_one.astype(jnp.float32) + summed).astype(jnp.bfloat16)
    return (results, new_state)


def solution(mesh):
    placed = (
        P("dp", ("kv", "tp")),
        P(None, "tp", "kv"),
        P(None, "tp", "kv"),
        P(None, "tp", "kv"),
        P(None, "tp", "kv"),
        P("tp"),
        P(),
        P(None, ("kv", "tp")),
        P(),
        P(),
        P(None, ("kv", "tp")),
        P(("kv", "tp"), None),
        P(("dp", "kv"), "tp", None, None),
    )
    return jax.shard_map(
        per_device,
        mesh=mesh,
        in_specs=placed,
        out_specs=(P("dp", ("kv", "tp")), P(("dp", "kv"), "tp", None, None)),
        check_vma=False,
    )
```

profile of v0, /device:TPU:0, one launch (start us, length us, event | category | flops | bytes accessed | tf_op | source)
XLA Modules:
  0.0 146.4 jit_solution(5957048308820464604)
XLA Ops:
  7.2 0.0 copy-start
  7.2 0.0 copy-start.4
  7.2 16.0 %all_gather.9 = bf16[8,4096]{1,0:T(8,128)(2,1)S(1)} all-gather(bf16[8,512]{1,0:T(8,128)(2,1)} %param.13), channel_id=1, replica_groups=mesh['dp'=4,'kv'=4,'tp'=2] {'kv','tp'}, dimensions={1}, use_global_device_ids=true | all-gather | bytes 73728 | tf_op jit(solution)/shard_map/all_gather | solution.py:31
  23.2 0.1 fusion.24
  23.4 2.0 %fusion.20 = bf16[8,256]{1,0:T(8,128)(2,1)S(1)} fusion(bf16[4096,1,256]{2,0,1:T(8,128)(2,1)} %param.17, bf16[8,4096]{1,0:T(8,128)(2,1)S(1)} %all_gather.9, f32[4096]{0:T(1024)} %param.21, f32[8]{0:T(128)S(1)} %add_rsqrt_fusion.2), kind=kOutput, calls=%fused_computation.16 | convolution fusion | flops 16910336 | bytes 2183200 | tf_op jit(solution)/shard_map/dot_general | solution.py:35
  25.4 0.6 all_to_all.46
  26.0 4.6 %all-to-all-start.3 = ((bf16[4,2,256]{2,1,0:T(2,128)(2,1)}), bf16[4,2,256]{2,1,0:T(2,128)(2,1)S(1)}, u32[]{:S(2)}, u32[]{:S(2)}) async-start(bf16[4,2,256]{2,1,0:T(2,128)(2,1)} %all_to_all.46), calls=%async_computation.3 | async-start | bytes 8192 | tf_op jit(solution)/shard_map/all_to_all | solution.py:43
  30.7 0.0 copy-done.4
  30.7 0.0 copy-start.2
  30.7 0.0 copy-start.3
  30.7 2.2 %fusion.14 = bf16[8,256]{1,0:T(8,128)(2,1)S(1)} fusion(bf16[4096,1,256]{2,0,1:T(8,128)(2,1)} %param.15, bf16[8,4096]{1,0:T(8,128)(2,1)S(1)} %all_gather.9, f32[4096]{0:T(1024)S(1)} %copy-done.4, f32[8]{0:T(128)S(1)} %add_rsqrt_fusion.2), kind=kOutput, calls=%fused_computation.14 | convolution fusion | flops 16910336 | bytes 2183200 | tf_op jit(solution)/shard_map/dot_general | solution.py:35
  32.8 0.1 copy-done.2
  32.9 0.0 copy-start.7
  32.9 0.4 fusion.17
  33.3 0.2 copy-done.3
  33.5 0.4 fusion.11
  33.9 0.0 copy-done.7
  33.9 0.0 copy-start.5
  34.0 0.6 all_to_all.42
  34.6 0.6 all_to_all.44
  35.2 0.6 all_to_all.40
  35.8 0.5 all-to-all-done.3
  36.2 4.6 %all-to-all-start = ((bf16[4,2,256]{2,1,0:T(2,128)(2,1)}), bf16[4,2,256]{2,1,0:T(2,128)(2,1)S(1)}, u32[]{:S(2)}, u32[]{:S(2)}) async-start(bf16[4,2,256]{2,1,0:T(2,128)(2,1)} %all_to_all.40), calls=%async_computation | async-start | bytes 8192 | tf_op jit(solution)/shard_map/all_to_all | solution.py:40
  40.9 5.6 %all-to-all-done = bf16[4,2,256]{2,1,0:T(2,128)(2,1)S(1)} async-done(((bf16[4,2,256]{2,1,0:T(2,128)(2,1)}), bf16[4,2,256]{2,1,0:T(2,128)(2,1)S(1)}, u32[]{:S(2)}, u32[]{:S(2)}) %all-to-all-start) | async-done | bytes 4128 | tf_op jit(solution)/shard_map/all_to_all | solution.py:40
  46.4 3.2 %all-to-all-start.2 = ((bf16[4,2,256]{2,1,0:T(2,128)(2,1)}), bf16[4,2,256]{2,1,0:T(2,128)(2,1)S(1)}, u32[]{:S(2)}, u32[]{:S(2)}) async-start(bf16[4,2,256]{2,1,0:T(2,128)(2,1)} %all_to_all.44), calls=%async_computation.2 | async-start | bytes 8192 | tf_op jit(solution)/shard_map/all_to_all | solution.py:42
  49.7 5.5 %all-to-all-done.2 = bf16[4,2,256]{2,1,0:T(2,128)(2,1)S(1)} async-done(((bf16[4,2,256]{2,1,0:T(2,128)(2,1)}), bf16[4,2,256]{2,1,0:T(2,128)(2,1)S(1)}, u32[]{:S(2)}, u32[]{:S(2)}) %all-to-all-start.2) | async-done | bytes 4128 | tf_op jit(solution)/shard_map/all_to_all | solution.py:42
  55.2 3.2 %all-to-all-start.1 = ((bf16[4,2,256]{2,1,0:T(2,128)(2,1)}), bf16[4,2,256]{2,1,0:T(2,128)(2,1)S(1)}, u32[]{:S(2)}, u32[]{:S(2)}) async-start(bf16[4,2,256]{2,1,0:T(2,128)(2,1)} %all_to_all.42), calls=%async_computation.1 | async-start | bytes 8192 | tf_op jit(solution)/shard_map/all_to_all | solution.py:41
  58.4 0.0 reduce-scatter.2.cloned.1.call-start
  58.6 5.4 %all-to-all-done.1 = bf16[4,2,256]{2,1,0:T(2,128)(2,1)S(1)} async-done(((bf16[4,2,256]{2,1,0:T(2,128)(2,1)}), bf16[4,2,256]{2,1,0:T(2,128)(2,1)S(1)}, u32[]{:S(2)}, u32[]{:S(2)}) %all-to-all-start.1) | async-done | bytes 4128 | tf_op jit(solution)/shard_map/all_to_all | solution.py:41
  64.0 1.8 %multiply_add_fusion = f32[2,8,128,128]{3,2,1,0:T(8,128)S(1)} fusion(f32[2,8,128,128]{3,2,1,0:T(8,128)} %param.25, f32[2,8,128]{2,1,0:T(8,128)S(1)} %reshape.112, f32[2,8,128]{2,1,0:T(8,128)S(1)} %get-tuple-element.2, f32[2,8,128]{2,1,0:T(8,128)S(1)} %get-tuple-element.3), kind=kLoop, calls=%fused_computation.17 | loop fusion | flops 786432 | bytes 2121728 | tf_op jit(solution)/shard_map/add | solution.py:58
  65.9 0.0 copy-start.1
  65.9 0.0 copy-start.6
  65.9 1.0 fusion.42
  66.9 0.1 multiply_reduce_fusion
  67.0 0.0 copy-done.8
  67.0 0.1 multiply_convert_fusion
  67.1 14.1 %all_gather.10 = bf16[2,8,1024]{2,0,1:T(2,128)(2,1)S(1)} all-gather(bf16[2,1,1024]{2,0,1:T(2,128)(2,1)S(1)} %convert_element_type.111), channel_id=1, replica_groups=mesh['dp'=4,'kv'=4,'tp'=2] {'kv','tp'}, dimensions={1}, use_global_device_ids=true | all-gather | bytes 36864 | tf_op jit(solution)/shard_map/all_gather | solution.py:63
  81.2 0.0 copy-done
  81.2 0.0 copy-done.5
  81.2 0.4 fusion.10
  81.6 14.0 %all_gather.11 = bf16[8,4096]{1,0:T(8,128)(2,1)S(1)} all-gather(bf16[8,512]{1,0:T(8,128)(2,1)S(1)} %fusion.10), channel_id=1, replica_groups=mesh['dp'=4,'kv'=4,'tp'=2] {'kv','tp'}, dimensions={1}, use_global_device_ids=true | all-gather | bytes 73728 | tf_op jit(solution)/shard_map/all_gather | solution.py:70
  95.6 0.1 fusion.27
  95.7 0.0 copy-done.6
  95.7 13.5 %fusion.23 = f32[8,4096]{1,0:T(8,128)} fusion(bf16[2048,4096]{1,0:T(8,128)(2,1)} %param.24, bf16[4096,2048]{1,0:T(8,128)(2,1)} %param.23, bf16[8,4096]{1,0:T(8,128)(2,1)S(1)} %all_gather.11, f32[4096]{0:T(1024)S(1)} %copy-done.6, f32[8]{0:T(128)S(1)} %add_rsqrt_fusion.1), kind=kOutput, calls=%fused_computation.18 | convolution fusion | flops 268615680 | bytes 33767456 | tf_op jit(solution)/shard_map/dot_general | solution.py:74
  109.3 0.0 copy-done.1
  109.3 0.0 reduce-scatter.2.cloned.1.call-update
  109.3 28.9 %reduce-scatter.2.cloned.1.call-done = f32[8,512]{1,0:T(8,128)} async-done(((f32[8,4096]{1,0:T(8,128)}), f32[8,512]{1,0:T(8,128)}) %reduce-scatter.2.cloned.1.call-update) | async-done | bytes 16400 | tf_op jit(solution)/shard_map/reduce_scatter | solution.py:75
  138.2 1.3 add_convert_fusion
  (21 shorter events, 0.2 us)
Async XLA Ops:
  7.2 74.0 %copy-start = (bf16[2048,512]{1,0:T(8,128)(2,1)S(1)}, bf16[2048,512]{1,0:T(8,128)(2,1)}, u32[]{:S(2)}) copy-start(bf16[2048,512]{1,0:T(8,128)(2,1)} %param.20) | copy-start | bytes 6291460
  7.2 23.5 %copy-start.4 = (f32[4096]{0:T(1024)S(1)}, f32[4096]{0:T(1024)}, u32[]{:S(2)}) copy-start(f32[4096]{0:T(1024)} %param.21) | copy-start | bytes 49156
  26.0 10.2 %all-to-all-start.3 = ((bf16[4,2,256]{2,1,0:T(2,128)(2,1)}), bf16[4,2,256]{2,1,0:T(2,128)(2,1)S(1)}, u32[]{:S(2)}, u32[]{:S(2)}) async-start(bf16[4,2,256]{2,1,0:T(2,128)(2,1)} %all_to_all.46), calls=%async_computation.3 | async-start | bytes 8192 | tf_op jit(solution)/shard_map/all_to_all | solution.py:43
  30.7 2.2 %copy-start.2 = (bf16[4096,1,256]{2,0,1:T(8,128)(2,1)S(1)}, bf16[4096,1,256]{2,0,1:T(8,128)(2,1)}, u32[]{:S(2)}) copy-start(bf16[4096,1,256]{2,0,1:T(8,128)(2,1)} %param.16) | copy-start | bytes 6291460
  30.7 2.9 %copy-start.3 = (bf16[4096,1,256]{2,0,1:T(8,128)(2,1)S(1)}, bf16[4096,1,256]{2,0,1:T(8,128)(2,1)}, u32[]{:S(2)}) copy-start(bf16[4096,1,256]{2,0,1:T(8,128)(2,1)} %param.14) | copy-start | bytes 6291460
  32.9 1.0 copy-start.7
  33.9 33.0 %copy-start.8 = (f32[128]{0:T(128)S(1)}, f32[128]{0:T(128)}, u32[]{:S(2)}) copy-start(f32[128]{0:T(128)} %param.19) | copy-start | bytes 1540
  33.9 47.3 %copy-start.5 = (bf16[8,512]{1,0:T(8,128)(2,1)S(1)}, bf16[8,512]{1,0:T(8,128)(2,1)}, u32[]{:S(2)}) copy-start(bf16[8,512]{1,0:T(8,128)(2,1)} %param.13) | copy-start | bytes 24580
  36.2 10.2 %all-to-all-start = ((bf16[4,2,256]{2,1,0:T(2,128)(2,1)}), bf16[4,2,256]{2,1,0:T(2,128)(2,1)S(1)}, u32[]{:S(2)}, u32[]{:S(2)}) async-start(bf16[4,2,256]{2,1,0:T(2,128)(2,1)} %all_to_all.40), calls=%async_computation | async-start | bytes 8192 | tf_op jit(solution)/shard_map/all_to_all | solution.py:40
  46.4 8.8 %all-to-all-start.2 = ((bf16[4,2,256]{2,1,0:T(2,128)(2,1)}), bf16[4,2,256]{2,1,0:T(2,128)(2,1)S(1)}, u32[]{:S(2)}, u32[]{:S(2)}) async-start(bf16[4,2,256]{2,1,0:T(2,128)(2,1)} %all_to_all.44), calls=%async_computation.2 | async-start | bytes 8192 | tf_op jit(solution)/shard_map/all_to_all | solution.py:42
  55.2 8.8 %all-to-all-start.1 = ((bf16[4,2,256]{2,1,0:T(2,128)(2,1)}), bf16[4,2,256]{2,1,0:T(2,128)(2,1)S(1)}, u32[]{:S(2)}, u32[]{:S(2)}) async-start(bf16[4,2,256]{2,1,0:T(2,128)(2,1)} %all_to_all.42), calls=%async_computation.1 | async-start | bytes 8192 | tf_op jit(solution)/shard_map/all_to_all | solution.py:41
  58.4 79.8 %reduce-scatter.2.cloned.1.call-start = ((), (), s32[]{:S(2)}) async-start(), calls=%async_computation.5 | async-start | bytes 147456 | tf_op jit(solution)/shard_map/reduce_scatter | solution.py:75
  65.9 43.4 %copy-start.1 = (f32[2,8,128,128]{3,2,1,0:T(8,128)}, f32[2,8,128,128]{3,2,1,0:T(8,128)S(1)}, u32[]{:S(2)}) copy-start(f32[2,8,128,128]{3,2,1,0:T(8,128)S(1)} %multiply_add_fusion) | copy-start | bytes 3145732
  65.9 29.9 %copy-start.6 = (f32[4096]{0:T(1024)S(1)}, f32[4096]{0:T(1024)}, u32[]{:S(2)}) copy-start(f32[4096]{0:T(1024)} %param.22) | copy-start | bytes 49156
Sparse Core Ops, SparseCore 0:
  109.4 28.7 reduce-scatter.1
where the time goes:
time: 147 us; the launch traced here: 146 us
  waiting for transfers between devices  45.9 us (31%)
  blocking collectives  44.1 us (30%)
  matrix products  19.9 us (14%)
  starting transfers between devices  15.7 us (11%)
  between operations  14.2 us (10%)
  other arithmetic  3.68 us (3%)
  local copies, waits for them, and re-layouts  2.83 us (2%)
    reduce_scatter x1, waiting for transfers between devices, per_device(): lax.psum_scatter(partial_terms, ('kv', 'tp'), scatter_dimension=1, tiled=...  28.9 us
    all_gather x1, blocking collectives, per_device(): full_rows = lax.all_gather(tokens, ('kv', 'tp'), axis=1, tiled=True)  16 us
    all_gather x1, blocking collectives, per_device(): gathered = lax.all_gather(branch, ('kv', 'tp'), axis=1, tiled=True)  14.1 us
    all_gather x1, blocking collectives, per_device(): whole_rows = lax.all_gather(residual_one, ('kv', 'tp'), axis=1, tiled=True)  14 us
    dot_general x1, matrix products, per_device(): partial_terms = jnp.dot(hidden, w_down, preferred_element_type=jnp.float32)  13.5 us
    all_to_all x1, waiting for transfers between devices, per_device(): lax.all_to_all(project(w_query), 'kv', split_axis=0, concat_axis=1, tiled...  5.57 us
    all_to_all x1, waiting for transfers between devices, per_device(): lax.all_to_all(project(w_input), 'kv', split_axis=0, concat_axis=1, tiled...  5.53 us
    all_to_all x1, waiting for transfers between devices, per_device(): lax.all_to_all(project(w_forget), 'kv', split_axis=0, concat_axis=1, tile...  5.41 us
  transfers between devices with their start and end apart: 5, of which 5 were waited for; matrix products, arithmetic and copies ran while one was open for 2% of the time, Pallas kernels for 0%

commit v1 on v0

--- a/solution.py
+++ b/solution.py
@@ -1,6 +1,10 @@
+import functools
+
 import jax
 import jax.numpy as jnp
 from jax import lax
+from jax.experimental import pallas as pl
+from jax.experimental.pallas import tpu as pltpu
 from jax.sharding import PartitionSpec as P
 
 EPSILON = 1e-06
@@ -77,6 +81,406 @@
     return (results, new_state)
 
 
+MESH = pl.DeviceIdType.MESH
+LANES = 128
+VMEM_BUDGET = 60 * 1024 * 1024
+PIECES = 4
+
+
+def fused_kernel(
+    n_kv,
+    n_tp,
+    tokens,
+    w_query,
+    w_forget,
+    w_input,
+    w_gate,
+    gate_floor,
+    head_gain,
+    w_out,
+    mix_gain,
+    ffn_gain,
+    w_up,
+    w_down,
+    state,
+    mixed,
+    new_state,
+    rows_all,
+    residual_all,
+    projections,
+    out_weight,
+    up_weight,
+    down_weight,
+    state_buf,
+    floor_buf,
+    head_gain_buf,
+    mix_gain_buf,
+    ffn_gain_buf,
+    normed,
+    proj_send,
+    proj_recv,
+    vectors,
+    head_buf,
+    branch_send,
+    branch_recv,
+    branch_all,
+    hidden,
+    sum_send,
+    sum_recv,
+    mixed_buf,
+    small_sem,
+    proj_sem,
+    out_sem,
+    up_sem,
+    down_sem,
+    state_sem,
+    result_sem,
+    send_sem,
+    recv_sem,
+):
+    group = n_kv * n_tp
+    kv = lax.axis_index("kv")
+    tp = lax.axis_index("tp")
+    me = kv * n_tp + tp
+    order = sorted(range(1, group), key=lambda r: -min(r, group - r))
+
+    def peer(r):
+        return lax.rem(me + r, group)
+
+    def device_of(index):
+        return {"kv": index // n_tp, "tp": lax.rem(index, n_tp)}
+
+    rows, width = tokens.shape
+    seqs, heads, size, _ = state.shape
+    proj_cols = w_query.shape[1]
+    heads_each = proj_cols // size
+    model = group * width
+
+    def load(source, target, sem):
+        copy = pltpu.make_async_copy(source, target, sem)
+        copy.start()
+        return copy
+
+    token_load = load(tokens, rows_all.at[me], small_sem.at[0])
+    mix_load = load(mix_gain, mix_gain_buf, small_sem.at[1])
+    proj_loads = [
+        load(w, projections.at[i], proj_sem.at[i])
+        for i, w in enumerate((w_query, w_forget, w_input, w_gate))
+    ]
+    floor_load = load(gate_floor, floor_buf, small_sem.at[2])
+    gain_load = load(head_gain, head_gain_buf, small_sem.at[3])
+    ffn_load = load(ffn_gain, ffn_gain_buf, small_sem.at[4])
+    state_load = load(state, state_buf, state_sem.at[0])
+    out_load = load(w_out, out_weight, out_sem.at[0])
+
+    def pieces(source, target, sems):
+        depth = source.shape[0] // PIECES
+        return [
+            load(
+                source.at[pl.ds(i * depth, depth)],
+                target.at[pl.ds(i * depth, depth)],
+                sems.at[i],
+            )
+            for i in range(PIECES)
+        ]
+
+    up_loads = pieces(w_up, up_weight, up_sem)
+    down_loads = pieces(w_down, down_weight, down_sem)
+
+    barrier = pltpu.get_barrier_semaphore()
+    for r in range(1, group):
+        pl.semaphore_signal(
+            barrier, inc=1, device_id=device_of(peer(r)), device_id_type=MESH
+        )
+    pl.semaphore_wait(barrier, group - 1)
+
+    def send(phase, slot, source, target, device):
+        copy = pltpu.make_async_remote_copy(
+            src_ref=source,
+            dst_ref=target,
+            send_sem=send_sem.at[phase, slot],
+            recv_sem=recv_sem.at[phase, slot],
+            device_id=device,
+            device_id_type=MESH,
+        )
+        copy.start()
+        return copy
+
+    def norm_rows(buffer, gain_ref):
+        parts = [buffer[s].astype(jnp.float32) for s in range(group)]
+        total = parts[0] * parts[0]
+        for part in parts[1:]:
+            total = total + part * part
+        scale = lax.rsqrt(jnp.sum(total, axis=-1, keepdims=True) / model + EPSILON)
+        for s in range(group):
+            columns = slice(s * width, (s + 1) * width)
+            normed[:, columns] = (parts[s] * scale * gain_ref[:, columns]).astype(
+                jnp.bfloat16
+            )
+
+    token_load.wait()
+    sends = [
+        send(0, r, rows_all.at[me], rows_all.at[me], device_of(peer(r))) for r in order
+    ]
+    mix_load.wait()
+    for copy in sends:
+        copy.wait_recv()
+    norm_rows(rows_all, mix_gain_buf)
+
+    for i in range(4):
+        proj_loads[i].wait()
+        product = jnp.dot(
+            normed[...], projections[i], preferred_element_type=jnp.float32
+        )
+        product = product.astype(jnp.bfloat16).astype(jnp.float32)
+        for s in range(n_kv):
+            for j in range(heads_each):
+                proj_send[s, i, j] = product[
+                    s * seqs : (s + 1) * seqs, j * size : (j + 1) * size
+                ]
+    exchange = []
+    for r in sorted(range(1, n_kv), key=lambda r: -min(r, n_kv - r)):
+        other = lax.rem(kv + r, n_kv)
+        exchange.append(
+            send(1, r, proj_send.at[other], proj_recv.at[kv], {"kv": other, "tp": tp})
+        )
+    own = pltpu.make_async_copy(proj_send.at[kv], proj_recv.at[kv], small_sem.at[5])
+    own.start()
+    floor_load.wait()
+    gain_load.wait()
+    state_load.wait()
+    own.wait()
+    for copy in exchange:
+        copy.wait_recv()
+
+    for i in range(4):
+        for s in range(n_kv):
+            for j in range(heads_each):
+                piece = proj_recv[s, i, j]
+                for b in range(seqs):
+                    row = b * heads + s * heads_each + j
+                    vectors[i, row : row + 1, :] = piece[b : b + 1, :]
+
+    floor = jnp.concatenate([floor_buf[...]] * seqs, axis=0)
+    forget = floor + (1.0 - floor) * jax.nn.sigmoid(vectors[1])
+    forget_t = forget.T
+    query_t = (vectors[0] * size ** (-0.5)).T
+    for b in range(seqs):
+        for h in range(heads):
+            row = b * heads + h
+            f = jnp.broadcast_to(forget_t[:, row : row + 1], (size, size))
+            q = jnp.broadcast_to(query_t[:, row : row + 1], (size, size))
+            value = vectors[2, row : row + 1, :]
+            updated = f * state_buf[b, h] + (1.0 - f) * value
+            state_buf[b, h] = updated
+            head_buf[row : row + 1, :] = jnp.sum(q * updated, axis=0, keepdims=True)
+    heads_out = head_buf[...]
+    gate = vectors[3]
+    branch = (
+        heads_out
+        * lax.rsqrt(jnp.mean(heads_out * heads_out, axis=-1, keepdims=True) + EPSILON)
+        * head_gain_buf[...]
+        * (gate * jax.nn.sigmoid(gate))
+    )
+    branch = branch.astype(jnp.bfloat16).astype(jnp.float32)
+    for b in range(seqs):
+        for h in range(heads):
+            row = b * heads + h
+            branch_send[b : b + 1, h * size : (h + 1) * size] = branch[row : row + 1, :]
+    branch_copies = [
+        send(2, r, branch_send, branch_recv.at[kv, tp], device_of(peer(r)))
+        for r in order
+    ]
+    own_branch = pltpu.make_async_copy(
+        branch_send, branch_recv.at[kv, tp], small_sem.at[6]
+    )
+    own_branch.start()
+    state_store = load(state_buf, new_state, result_sem.at[0])
+    out_load.wait()
+    own_branch.wait()
+    for copy in branch_copies:
+        copy.wait_recv()
+    for s in range(n_kv):
+        for t in range(n_tp):
+            branch_all[
+                s * seqs : (s + 1) * seqs, t * heads * size : (t + 1) * heads * size
+            ] = branch_recv[s, t]
+    projected = jnp.dot(
+        branch_all[...].astype(jnp.bfloat16),
+        out_weight[...],
+        preferred_element_type=jnp.float32,
+    )
+    residual_all[me] = (rows_all[me].astype(jnp.float32) + projected).astype(
+        jnp.bfloat16
+    )
+    residual_copies = [
+        send(3, r, residual_all.at[me], residual_all.at[me], device_of(peer(r)))
+        for r in order
+    ]
+    ffn_load.wait()
+    for copy in residual_copies:
+        copy.wait_recv()
+    norm_rows(residual_all, ffn_gain_buf)
+
+    for copy in up_loads:
+        copy.wait()
+    hidden_cols = w_up.shape[1]
+    step = min(512, hidden_cols)
+
+    def up_step(j, carry):
+        columns = pl.ds(pl.multiple_of(j * step, step), step)
+        upward = jnp.dot(
+            normed[...], up_weight[:, columns], preferred_element_type=jnp.float32
+        )
+        upward = jnp.maximum(upward, 0.0)
+        hidden[:, columns] = (upward * upward).astype(jnp.bfloat16)
+        return carry
+
+    lax.fori_loop(0, hidden_cols // step, up_step, 0)
+
+    for copy in down_loads:
+        copy.wait()
+
+    def down(index):
+        columns = pl.ds(pl.multiple_of(index * width, width), width)
+        return jnp.dot(
+            hidden[...], down_weight[:, columns], preferred_element_type=jnp.float32
+        )
+
+    sum_copies = []
+    for r in order:
+        sum_send[r] = down(peer(r)).astype(jnp.bfloat16)
+        sum_copies.append(
+            send(4, r, sum_send.at[r], sum_recv.at[r], device_of(peer(r)))
+        )
+    total = down(me)
+    for copy in sum_copies:
+        copy.wait_recv()
+    for r in range(1, group):
+        total = total + sum_recv[r].astype(jnp.float32)
+    mixed_buf[...] = (residual_all[me].astype(jnp.float32) + total).astype(jnp.bfloat16)
+    mixed_store = load(mixed_buf, mixed, result_sem.at[1])
+    for copy in sends + exchange + branch_copies + residual_copies + sum_copies:
+        copy.wait_send()
+    state_store.wait()
+    mixed_store.wait()
+
+
+def fused_scratch(n_kv, n_tp, tokens, w_query, w_out, w_up, w_down, state):
+    group = n_kv * n_tp
+    rows, width = tokens.shape
+    seqs, heads, size, _ = state.shape
+    heads_each = w_query.shape[2] // size
+    bf16, f32 = jnp.bfloat16, jnp.float32
+    return [
+        pltpu.VMEM((group, rows, width), bf16),
+        pltpu.VMEM((group, rows, width), bf16),
+        pltpu.VMEM((4, w_query.shape[0], w_query.shape[2]), bf16),
+        pltpu.VMEM(w_out.shape, bf16),
+        pltpu.VMEM(w_up.shape, bf16),
+        pltpu.VMEM(w_down.shape, bf16),
+        pltpu.VMEM(state.shape, f32),
+        pltpu.VMEM((heads, size), f32),
+        pltpu.VMEM((1, size), f32),
+        pltpu.VMEM((1, group * width), f32),
+        pltpu.VMEM((1, group * width), f32),
+        pltpu.VMEM((rows, group * width), bf16),
+        pltpu.VMEM((n_kv, 4, heads_each, seqs, size), f32),
+        pltpu.VMEM((n_kv, 4, heads_each, seqs, size), f32),
+        pltpu.VMEM((4, seqs * heads, size), f32),
+        pltpu.VMEM((seqs * heads, size), f32),
+        pltpu.VMEM((seqs, heads * size), f32),
+        pltpu.VMEM((n_kv, n_tp, seqs, heads * size), f32),
+        pltpu.VMEM((rows, n_tp * heads * size), f32),
+        pltpu.VMEM((rows, w_up.shape[1]), bf16),
+        pltpu.VMEM((group, rows, width), bf16),
+        pltpu.VMEM((group, rows, width), bf16),
+        pltpu.VMEM((rows, width), bf16),
+        pltpu.SemaphoreType.DMA((7,)),
+        pltpu.SemaphoreType.DMA((4,)),
+        pltpu.SemaphoreType.DMA((1,)),
+        pltpu.SemaphoreType.DMA((PIECES,)),
+        pltpu.SemaphoreType.DMA((PIECES,)),
+        pltpu.SemaphoreType.DMA((1,)),
+        pltpu.SemaphoreType.DMA((2,)),
+        pltpu.SemaphoreType.DMA((5, group)),
+        pltpu.SemaphoreType.DMA((5, group)),
+    ]
+
+
+def fused(
+    tokens,
+    w_query,
+    w_forget,
+    w_input,
+    w_output_gate,
+    gate_floor,
+    head_gain,
+    w_out,
+    mix_gain,
+    ffn_gain,
+    w_up,
+    w_down,
+    state,
+):
+    n_kv = lax.axis_size("kv")
+    n_tp = lax.axis_size("tp")
+    anywhere = pl.BlockSpec(memory_space=pl.ANY)
+    size = state.shape[2]
+    return pl.pallas_call(
+        functools.partial(fused_kernel, n_kv, n_tp),
+        out_shape=(
+            jax.ShapeDtypeStruct(tokens.shape, jnp.bfloat16),
+            jax.ShapeDtypeStruct(state.shape, jnp.float32),
+        ),
+        in_specs=[anywhere] * 13,
+        out_specs=(anywhere, anywhere),
+        scratch_shapes=fused_scratch(
+            n_kv, n_tp, tokens, w_query, w_out, w_up, w_down, state
+        ),
+        compiler_params=pltpu.CompilerParams(
+            collective_id=0, has_side_effects=True, vmem_limit_bytes=VMEM_BUDGET
+        ),
+    )(
+        tokens,
+        w_query[:, 0, :],
+        w_forget[:, 0, :],
+        w_input[:, 0, :],
+        w_output_gate[:, 0, :],
+        gate_floor.reshape(state.shape[1], size),
+        head_gain.reshape(1, size),
+        w_out,
+        mix_gain.reshape(1, -1),
+        ffn_gain.reshape(1, -1),
+        w_up,
+        w_down,
+        state,
+    )
+
+
+def dispatch(*operands):
+    tokens, w_query, w_out, w_up, w_down, state = (
+        operands[0],
+        operands[1],
+        operands[7],
+        operands[10],
+        operands[11],
+        operands[12],
+    )
+    weights = 2 * (4 * w_query.size + w_out.size + w_up.size + w_down.size)
+    held = weights + 4 * state.size + 64 * tokens.size * lax.axis_size("kv")
+    size = state.shape[2]
+    if (
+        held <= VMEM_BUDGET
+        and size == LANES
+        and w_query.shape[2] % size == 0
+        and tokens.shape[0] == lax.axis_size("kv") * state.shape[0]
+        and tokens.shape[0] <= 64
+    ):
+        return fused(*operands)
+    return per_device(*operands)
+
+
 def solution(mesh):
     placed = (
         P("dp", ("kv", "tp")),
@@ -94,7 +498,7 @@
         P(("dp", "kv"), "tp", None, None),
     )
     return jax.shard_map(
-        per_device,
+        dispatch,
         mesh=mesh,
         in_specs=placed,
         out_specs=(P("dp", ("kv", "tp")), P(("dp", "kv"), "tp", None, None)),

time: 147 us -> 40.2 us (0.27)
  waiting for transfers between devices: 45.9 us -> 0 us
  blocking collectives: 44.1 us -> 0 us
  Pallas kernels: 0 us -> 35.7 us
  matrix products: 19.9 us -> 0 us
  starting transfers between devices: 15.7 us -> 0 us
  between operations: 14.2 us -> 0.64 us
  other arithmetic: 3.68 us -> 0 us
    all_gather x3 -> x0, blocking collectives: 44.1 us -> none  [the longest x1 16 us: per_device(): full_rows = lax.all_gather(tokens, ('kv', 'tp'), axis=1, tiled=True)]
    pallas_call x0 -> x1, Pallas kernels: none -> 35.7 us  [fused(): pl.pallas_call(functools.partial(fused_kernel, n_kv, n_tp), out_shape=(ja...]
    reduce_scatter x1 -> x0, waiting for transfers between devices: 28.9 us -> none  [per_device(): lax.psum_scatter(partial_terms, ('kv', 'tp'), scatter_dimension=1, tiled=...]
    dot_general x7 -> x0, matrix products: 19.9 us -> none  [the longest x1 13.5 us: per_device(): partial_terms = jnp.dot(hidden, w_down, preferred_element_type=jnp.float32)]
    all_to_all x4 -> x0, waiting for transfers between devices: 17 us -> none  [the longest x1 5.57 us: per_device(): lax.all_to_all(project(w_query), 'kv', split_axis=0, concat_axis=1, tiled...]
    all_to_all x4 -> x0, starting transfers between devices: 15.7 us -> none  [the longest x1 4.64 us: per_device(): lax.all_to_all(project(w_output_gate), 'kv', split_axis=0, concat_axis=1,...]
    unnamed x19 -> x2, local copies, waits for them, and re-layouts: 0.32 us -> 3.59 us
    all_to_all x4 -> x0, local copies, waits for them, and re-layouts: 2.41 us -> none  [the longest x1 0.61 us: per_device(): lax.all_to_all(project(w_output_gate), 'kv', split_axis=0, concat_axis=1,...]
  transfers between devices with their start and end apart: 5 -> 0, of which waited for: 5 -> 0; matrix products, arithmetic and copies ran while one was open for 2% -> 0% of each run, Pallas kernels for 0% -> 0%
where the time goes in v1:
time: 40.2 us; the launch traced here: 39.9 us
  Pallas kernels  35.7 us (89%)
  local copies, waits for them, and re-layouts  3.59 us (9%)
  between operations  0.64 us (2%)
    pallas_call x1, Pallas kernels, fused(): pl.pallas_call(functools.partial(fused_kernel, n_kv, n_tp), out_shape=(ja...  35.7 us
    unnamed x2, local copies, waits for them, and re-layouts  3.59 us

profile of v1, /device:TPU:0, one launch (start us, length us, event | category | flops | bytes accessed | tf_op | source)
XLA Modules:
  0.0 39.9 jit_solution(14543679421789491545)
XLA Ops:
  0.6 35.7 %shard_map.140 = (bf16[8,512]{1,0:T(8,128)(2,1)}, f32[2,8,128,128]{3,2,1,0:T(8,128)}) custom-call(bf16[8,512]{1,0:T(8,128)(2,1)} %tokens.1, bf16[4096,256]{1,0:T(8,128)(2,1)} %bitcast.8, bf16[4096,256]{1,0:T(8,128)(2,1)} %bitcast.9, bf16[4096,256]{1,0:T(8,128)(2,1)} %bitcast.10, bf16[4096,256]{1,0:T(8,128)(2,1)} %bitcast.11, f32[8,128]{1,0:T(8,128)} %bitcast.14, ...), custom_call_target="tpu_custom_call" | custom-call | tf_op jit(solution)/shard_map/pallas_call | solution.py:430
  36.4 1.3 %copy.17 = bf16[8,512]{1,0:T(8,128)(2,1)} copy(bf16[8,512]{1,0:T(8,128)(2,1)} %get-tuple-element.4) | data formatting | bytes 16384
  37.6 2.3 %copy.18 = f32[2,8,128,128]{3,2,1,0:T(8,128)} copy(f32[2,8,128,128]{3,2,1,0:T(8,128)} %get-tuple-element.5) | data formatting | bytes 2097152

commit v2 on v1

--- a/solution.py
+++ b/solution.py
@@ -116,7 +116,6 @@
     head_gain_buf,
     mix_gain_buf,
     ffn_gain_buf,
-    normed,
     proj_send,
     proj_recv,
     vectors,
@@ -127,14 +126,12 @@
     hidden,
     sum_send,
     sum_recv,
-    mixed_buf,
     small_sem,
     proj_sem,
     out_sem,
     up_sem,
     down_sem,
     state_sem,
-    result_sem,
     send_sem,
     recv_sem,
 ):
@@ -184,9 +181,6 @@
             for i in range(PIECES)
         ]
 
-    up_loads = pieces(w_up, up_weight, up_sem)
-    down_loads = pieces(w_down, down_weight, down_sem)
-
     barrier = pltpu.get_barrier_semaphore()
     for r in range(1, group):
         pl.semaphore_signal(
@@ -206,32 +200,45 @@
         copy.start()
         return copy
 
-    def norm_rows(buffer, gain_ref):
-        parts = [buffer[s].astype(jnp.float32) for s in range(group)]
-        total = parts[0] * parts[0]
-        for part in parts[1:]:
-            total = total + part * part
-        scale = lax.rsqrt(jnp.sum(total, axis=-1, keepdims=True) / model + EPSILON)
-        for s in range(group):
-            columns = slice(s * width, (s + 1) * width)
-            normed[:, columns] = (parts[s] * scale * gain_ref[:, columns]).astype(
-                jnp.bfloat16
-            )
+    def gathered_dot(buffer, gain_ref, copies, weight_of):
+        arrivals = [(me, None)] + [
+            (lax.rem(me + group - r, group), copy)
+            for r, copy in reversed(list(zip(order, copies)))
+        ]
+        sums = None
+        squares = None
+        for source, copy in arrivals:
+            if copy is not None:
+                copy.wait_recv()
+            columns = pl.ds(pl.multiple_of(source * width, width), width)
+            part = buffer[source].astype(jnp.float32)
+            square = part * part
+            squares = square if squares is None else squares + square
+            scaled = (part * gain_ref[:, columns]).astype(jnp.bfloat16)
+            terms = [
+                jnp.dot(scaled, block, preferred_element_type=jnp.float32)
+                for block in weight_of(columns)
+            ]
+            sums = terms if sums is None else [a + b for a, b in zip(sums, terms)]
+        scale = lax.rsqrt(jnp.sum(squares, axis=-1, keepdims=True) / model + EPSILON)
+        return [total * scale for total in sums]
 
     token_load.wait()
     sends = [
         send(0, r, rows_all.at[me], rows_all.at[me], device_of(peer(r))) for r in order
     ]
     mix_load.wait()
-    for copy in sends:
-        copy.wait_recv()
-    norm_rows(rows_all, mix_gain_buf)
-
-    for i in range(4):
-        proj_loads[i].wait()
-        product = jnp.dot(
-            normed[...], projections[i], preferred_element_type=jnp.float32
-        )
+    for copy in proj_loads:
+        copy.wait()
+    up_loads = pieces(w_up, up_weight, up_sem)
+    down_loads = pieces(w_down, down_weight, down_sem)
+    products = gathered_dot(
+        rows_all,
+        mix_gain_buf,
+        sends,
+        lambda rows_at: [projections[i, rows_at, :] for i in range(4)],
+    )
+    for i, product in enumerate(products):
         product = product.astype(jnp.bfloat16).astype(jnp.float32)
         for s in range(n_kv):
             for j in range(heads_each):
@@ -272,7 +279,7 @@
             q = jnp.broadcast_to(query_t[:, row : row + 1], (size, size))
             value = vectors[2, row : row + 1, :]
             updated = f * state_buf[b, h] + (1.0 - f) * value
-            state_buf[b, h] = updated
+            new_state[b, h] = updated
             head_buf[row : row + 1, :] = jnp.sum(q * updated, axis=0, keepdims=True)
     heads_out = head_buf[...]
     gate = vectors[3]
@@ -295,7 +302,6 @@
         branch_send, branch_recv.at[kv, tp], small_sem.at[6]
     )
     own_branch.start()
-    state_store = load(state_buf, new_state, result_sem.at[0])
     out_load.wait()
     own_branch.wait()
     for copy in branch_copies:
@@ -318,25 +324,16 @@
         for r in order
     ]
     ffn_load.wait()
-    for copy in residual_copies:
-        copy.wait_recv()
-    norm_rows(residual_all, ffn_gain_buf)
-
     for copy in up_loads:
         copy.wait()
-    hidden_cols = w_up.shape[1]
-    step = min(512, hidden_cols)
-
-    def up_step(j, carry):
-        columns = pl.ds(pl.multiple_of(j * step, step), step)
-        upward = jnp.dot(
-            normed[...], up_weight[:, columns], preferred_element_type=jnp.float32
-        )
-        upward = jnp.maximum(upward, 0.0)
-        hidden[:, columns] = (upward * upward).astype(jnp.bfloat16)
-        return carry
-
-    lax.fori_loop(0, hidden_cols // step, up_step, 0)
+    (upward,) = gathered_dot(
+        residual_all,
+        ffn_gain_buf,
+        residual_copies,
+        lambda rows_at: [up_weight[rows_at, :]],
+    )
+    upward = jnp.maximum(upward, 0.0)
+    hidden[...] = (upward * upward).astype(jnp.bfloat16)
 
     for copy in down_loads:
         copy.wait()
@@ -358,12 +355,9 @@
         copy.wait_recv()
     for r in range(1, group):
         total = total + sum_recv[r].astype(jnp.float32)
-    mixed_buf[...] = (residual_all[me].astype(jnp.float32) + total).astype(jnp.bfloat16)
-    mixed_store = load(mixed_buf, mixed, result_sem.at[1])
+    mixed[...] = (residual_all[me].astype(jnp.float32) + total).astype(jnp.bfloat16)
     for copy in sends + exchange + branch_copies + residual_copies + sum_copies:
         copy.wait_send()
-    state_store.wait()
-    mixed_store.wait()
 
 
 def fused_scratch(n_kv, n_tp, tokens, w_query, w_out, w_up, w_down, state):
@@ -384,7 +378,6 @@
         pltpu.VMEM((1, size), f32),
         pltpu.VMEM((1, group * width), f32),
         pltpu.VMEM((1, group * width), f32),
-        pltpu.VMEM((rows, group * width), bf16),
         pltpu.VMEM((n_kv, 4, heads_each, seqs, size), f32),
         pltpu.VMEM((n_kv, 4, heads_each, seqs, size), f32),
         pltpu.VMEM((4, seqs * heads, size), f32),
@@ -395,14 +388,12 @@
         pltpu.VMEM((rows, w_up.shape[1]), bf16),
         pltpu.VMEM((group, rows, width), bf16),
         pltpu.VMEM((group, rows, width), bf16),
-        pltpu.VMEM((rows, width), bf16),
         pltpu.SemaphoreType.DMA((7,)),
         pltpu.SemaphoreType.DMA((4,)),
         pltpu.SemaphoreType.DMA((1,)),
         pltpu.SemaphoreType.DMA((PIECES,)),
         pltpu.SemaphoreType.DMA((PIECES,)),
         pltpu.SemaphoreType.DMA((1,)),
-        pltpu.SemaphoreType.DMA((2,)),
         pltpu.SemaphoreType.DMA((5, group)),
         pltpu.SemaphoreType.DMA((5, group)),
     ]
@@ -426,15 +417,16 @@
     n_kv = lax.axis_size("kv")
     n_tp = lax.axis_size("tp")
     anywhere = pl.BlockSpec(memory_space=pl.ANY)
+    in_vmem = pl.BlockSpec(memory_space=pltpu.VMEM)
     size = state.shape[2]
     return pl.pallas_call(
         functools.partial(fused_kernel, n_kv, n_tp),
         out_shape=(
-            jax.ShapeDtypeStruct(tokens.shape, jnp.bfloat16),
-            jax.ShapeDtypeStruct(state.shape, jnp.float32),
+            pltpu.VMEM(tokens.shape, jnp.bfloat16),
+            pltpu.VMEM(state.shape, jnp.float32),
         ),
         in_specs=[anywhere] * 13,
-        out_specs=(anywhere, anywhere),
+        out_specs=(in_vmem, in_vmem),
         scratch_shapes=fused_scratch(
             n_kv, n_tp, tokens, w_query, w_out, w_up, w_down, state
         ),

time: 40.2 us -> 33 us (0.82)
  Pallas kernels: 35.7 us -> 30.6 us
  local copies, waits for them, and re-layouts: 3.59 us -> 1.57 us
    pallas_call x1, Pallas kernels: 35.7 us -> 30.6 us  [fused(): pl.pallas_call(functools.partial(fused_kernel, n_kv, n_tp), out_shape=(pl...]
    unnamed x2, local copies, waits for them, and re-layouts: 3.59 us -> 1.57 us
where the time goes in v2:
time: 33 us; the launch traced here: 32.8 us
  Pallas kernels  30.6 us (93%)
  local copies, waits for them, and re-layouts  1.57 us (5%)
  between operations  0.64 us (2%)
    pallas_call x1, Pallas kernels, fused(): pl.pallas_call(functools.partial(fused_kernel, n_kv, n_tp), out_shape=(pl...  30.6 us
    unnamed x2, local copies, waits for them, and re-layouts  1.57 us

profile of v2, /device:TPU:0, one launch (start us, length us, event | category | flops | bytes accessed | tf_op | source)
XLA Modules:
  0.0 32.8 jit_solution(2155676259671834132)
XLA Ops:
  0.6 30.6 %shard_map.140 = (bf16[8,512]{1,0:T(8,128)(2,1)S(1)}, f32[2,8,128,128]{3,2,1,0:T(8,128)S(1)}) custom-call(bf16[8,512]{1,0:T(8,128)(2,1)} %tokens.1, bf16[4096,256]{1,0:T(8,128)(2,1)} %bitcast.8, bf16[4096,256]{1,0:T(8,128)(2,1)} %bitcast.9, bf16[4096,256]{1,0:T(8,128)(2,1)} %bitcast.10, bf16[4096,256]{1,0:T(8,128)(2,1)} %bitcast.11, f32[8,128]{1,0:T(8,128)} %bitcast.14, ...), custom_call_target="tpu_custom_call" | custom-call | tf_op jit(solution)/shard_map/pallas_call | solution.py:422
  31.2 0.6 %copy.17 = bf16[8,512]{1,0:T(8,128)(2,1)} copy(bf16[8,512]{1,0:T(8,128)(2,1)S(1)} %get-tuple-element.2) | data formatting | bytes 16384
  31.8 1.0 %copy.18 = f32[2,8,128,128]{3,2,1,0:T(8,128)} copy(f32[2,8,128,128]{3,2,1,0:T(8,128)S(1)} %get-tuple-element.3) | data formatting | bytes 2097152
